TPU v7x, 32 devices: a whole 2x2x4 slice. The times are simulated.
32 devices in a mesh: ep: 8 (over z, core), tp: 4 (over y, x).
Axes of the slice: x: 2, y: 2, z: 4, core: 2. Of those that a mesh axis runs over, the one named last changes fastest.
Arguments:
- tokens: bfloat16 [2048, 2048], P('ep'), may hold values from -6 to 6
- norm_gain: float32 [2048], replicated, may hold values from 0.1 to 1.9
- route_ids: int32 [2048, 4], P('ep'), may hold values from 0 to 15, all different within a row; in each aligned block of 256 rows (0 to 255, 256 to 511, ...) at most 96 rows name the same one
- route_weights: float32 [2048, 4], P('ep'), may hold values from 0.1 to 1
- w_gate: bfloat16 [16, 2048, 2048], P('ep', None, 'tp'), may hold values from -0.33007812 to 0.33007812
- w_up: bfloat16 [16, 2048, 2048], P('ep', None, 'tp'), may hold values from -0.33007812 to 0.33007812
- w_down: bfloat16 [16, 2048, 2048], P('ep', None, 'tp'), may hold values from -0.026489258 to 0.026489258
Outputs:
- mixed_out: bfloat16 [2048, 2048], P('ep', 'tp')
Inputs may be any that keep to these rules, and one draw needn't show every extreme that they name: `route_ids`: each token names 4 different experts. Within the tokens of one index of ep (aligned blocks of 256 tokens) no expert is named more than 96 times, a bound that some block reaches.
All inputs are finite; a program needn't handle non-finite values.
Results may differ from a plain program's by a relative error of at most 0.007.
Values may be sent and summed in bfloat16 or wider, within the bound.
A program may use at most 64 MiB of HBM per device.

v0:
```python
import functools
import jax
import jax.numpy as jnp
from jax import lax
from jax.experimental import pallas as pl
from jax.experimental.pallas import tpu as pltpu
from jax.sharding import PartitionSpec as P

swiglu_limit = 7.0
swiglu_alpha = 1.702
norm_eps = 1e-05


def clamped_units(gate_pre, up_pre):
    capped = jnp.minimum(gate_pre, swiglu_limit)
    linear = jnp.clip(up_pre, -swiglu_limit, swiglu_limit)
    return capped * jax.nn.sigmoid(swiglu_alpha * capped) * (linear + 1.0)


def expert_work(outgoing, gate_weight, up_weight, down_weight):
    received = lax.all_to_all(outgoing, "ep", split_axis=1, concat_axis=1, tiled=True)
    local_count, sources, capacity, columns = received.shape
    row_count = sources * capacity
    row_block = received.reshape(local_count, row_count, columns)
    shard_piece = lax.all_gather(row_block, "tp", axis=2, tiled=True)
    gate_sum = jnp.einsum(
        "lrd,ldf->lrf", shard_piece, gate_weight, preferred_element_type=jnp.float32
    )
    up_sum = jnp.einsum("lrd,ldf->lrf", shard_piece, up_weight, preferred_element_type=jnp.float32)
    activation = clamped_units(gate_sum, up_sum).astype(jnp.bfloat16)
    out_cols = down_weight.shape[2]
    result = jnp.einsum(
        "lrf,lfd->lrd",
        lax.all_gather(activation, "tp", axis=2, tiled=True),
        down_weight,
        preferred_element_type=jnp.float32,
    )
    result = result.astype(jnp.bfloat16).reshape(local_count, sources, capacity, out_cols)
    return lax.all_to_all(result, "ep", split_axis=1, concat_axis=1, tiled=True)


def per_device(tokens, norm_gain, route_ids, route_weights, w_gate, w_up, w_down):
    local_count = w_gate.shape[0]
    sources = lax.axis_size("ep")
    tp_count = lax.axis_size("tp")
    width = tokens.shape[1]
    columns = width // tp_count
    experts = local_count * sources
    tok_rows, top_count = route_ids.shape
    capacity = 3 * tok_rows * top_count // (2 * experts)
    values = tokens.astype(jnp.float32)
    row_mean = jnp.mean(values, axis=1, keepdims=True)
    centred = values - row_mean
    row_var = jnp.mean(centred * centred, axis=1, keepdims=True)
    offset = lax.axis_index("tp") * columns
    own_cols = lax.dynamic_slice_in_dim(centred, offset, columns, 1)
    own_gain = lax.dynamic_slice_in_dim(norm_gain, offset, columns, 0)
    normed = (own_cols * lax.rsqrt(row_var + norm_eps) * own_gain).astype(jnp.bfloat16)
    flat_ids = route_ids.reshape(-1)
    matches = (flat_ids[:, None] == jnp.arange(experts, dtype=jnp.int32)[None, :]).astype(jnp.int32)
    earlier = jnp.cumsum(matches, axis=0) - matches
    slot_index = jnp.sum(earlier * matches, axis=1)
    position = (
        flat_ids % local_count * (sources * capacity)
        + flat_ids // local_count * capacity
        + slot_index
    )
    buffer_rows = local_count * sources * capacity
    placed = (
        position.reshape(tok_rows, top_count)[:, :, None]
        == jnp.arange(buffer_rows, dtype=jnp.int32)[None, None, :]
    )
    placement_matrix = jnp.any(placed, axis=1).astype(jnp.bfloat16)
    outgoing = jnp.einsum("tp,td->pd", placement_matrix, normed, preferred_element_type=jnp.float32)
    outgoing = outgoing.astype(jnp.bfloat16).reshape(local_count, sources, capacity, columns)
    returned = jnp.concatenate(
        [
            expert_work(
                outgoing[number : number + 1],
                w_gate[number : number + 1],
                w_up[number : number + 1],
                w_down[number : number + 1],
            )
            for number in range(local_count)
        ],
        axis=0,
    )
    flat_out = returned.reshape(buffer_rows, columns)
    picked = flat_out[position].reshape(tok_rows, top_count, columns).astype(jnp.float32)
    return jnp.sum(picked * route_weights[:, :, None], axis=1).astype(jnp.bfloat16)


def layer_kernel(
    capacity,
    tokens_ref,
    gain_ref,
    meta_ref,
    gate_hbm,
    up_hbm,
    down_hbm,
    out_ref,
    gate_w,
    up_w,
    down_w,
    normed_ref,
    toks,
    meta_in,
    rows,
    acts,
    weighted,
    pair_out,
    pair_in,
    back_out,
    back_in,
    total_ref,
    weight_sem,
    local_sem,
    meta_send,
    meta_recv,
    line_send,
    line_recv,
    side_send,
    side_recv,
    pair_send,
    pair_recv,
    act_send,
    act_recv,
    sum_send,
    sum_recv,
    back_send,
    back_recv,
):
    sources = meta_ref.shape[0]
    chips = sources // 2
    local_count = gate_w.shape[0]
    units = gate_w.shape[2]
    tok_rows = normed_ref.shape[1]
    me = lax.axis_index("ep")
    tp = lax.axis_index("tp")
    z, core = me // 2, me % 2
    y, x = tp // 2, tp % 2
    tp_x = y * 2 + (1 - x)
    tp_y = (1 - y) * 2 + x
    tp_xy = (1 - y) * 2 + (1 - x)
    mate = z * 2 + (1 - core)
    own_half = (x + y) % 2

    def partner(k):
        chosen_chip = 0 * z
        for at in range(chips):
            order = sorted(range(chips), key=lambda c: (abs(c - at), c))
            gap = (z - at) * (z - at)
            chosen_chip = chosen_chip + order[k] * (1 - (gap + chips * chips - 1) // (chips * chips))
        return chosen_chip

    def place(ep, column):
        return {"ep": ep, "tp": column}

    def remote(source, target, send, recv, where):
        return pltpu.make_async_remote_copy(
            src_ref=source,
            dst_ref=target,
            send_sem=send,
            recv_sem=recv,
            device_id=where,
            device_id_type=pl.DeviceIdType.MESH,
        )

    loads = []
    for n, (hbm, vmem) in enumerate(((gate_hbm, gate_w), (up_hbm, up_w), (down_hbm, down_w))):
        loads.append(pltpu.make_async_copy(hbm, vmem, weight_sem.at[n]))
        loads[-1].start()
    own_meta = pltpu.make_async_copy(meta_ref.at[me], meta_in.at[me], local_sem.at[1])
    own_meta.start()

    barrier = pltpu.get_barrier_semaphore()
    for d in range(1, sources):
        pl.semaphore_signal(
            barrier, inc=1, device_id=place((me + d) % sources, tp), device_id_type=pl.DeviceIdType.MESH
        )
    for column in (tp_x, tp_y):
        pl.semaphore_signal(
            barrier, inc=1, device_id=place(me, column), device_id_type=pl.DeviceIdType.MESH
        )

    band = 32

    @pl.loop(0, tok_rows // band)
    def _(n):
        at = pl.ds(pl.multiple_of(n * band, band), band)
        values = tokens_ref[at, :].astype(jnp.float32)
        centred = values - jnp.mean(values, axis=1, keepdims=True)
        row_var = jnp.mean(centred * centred, axis=1, keepdims=True)
        normal = (centred * lax.rsqrt(row_var + norm_eps) * gain_ref[...]).astype(jnp.bfloat16)
        step = normed_ref.shape[2]
        for h in range(normed_ref.shape[0]):
            normed_ref[h, at, :] = normal[:, h * step : (h + 1) * step]

    pl.semaphore_wait(barrier, sources + 1)
    own_tok = pltpu.make_async_copy(normed_ref, toks.at[me], local_sem.at[0])
    own_tok.start()

    pending = []

    def go(copy):
        copy.start()
        pending.append(copy)
        return copy

    metas = [
        go(
            remote(
                meta_ref.at[(me + d) % sources],
                meta_in.at[me],
                meta_send.at[d],
                meta_recv.at[d],
                place((me + d) % sources, tp),
            )
        )
        for d in range(1, sources)
    ]
    own_pair = go(
        remote(normed_ref, toks.at[me], pair_send.at[0], pair_recv.at[0], place(mate, tp))
    )
    def line(chip, up, distance):
        piece = toks.at[chip * 2 + core, own_half]
        return remote(
            normed_ref.at[own_half] if distance is None else piece,
            piece,
            line_send.at[up, chip],
            line_recv.at[up, chip],
            place((z + 2 * up - 1) * 2 + core, tp),
        )

    @pl.when(z < chips - 1)
    def _():
        line(z, 1, None).start()

    @pl.when(z > 0)
    def _():
        line(z, 0, None).start()

    def upward(chip):
        return (chips + z - chip - 1) // chips

    def goes_on(chip):
        ahead = z + 2 * upward(chip) - 1
        return jnp.logical_and(ahead >= 0, ahead < chips)

    pairs, sides, half_pairs = {}, {}, {}
    cut_rows = tok_rows // 2

    def spread_line(k):
        chip = partner(k)
        src = chip * 2 + core
        up = upward(chip)
        line(chip, up, k).wait_recv()

        @pl.when(goes_on(chip))
        def _():
            line(chip, up, k).start()

        sides[k] = []
        for n, column in enumerate((tp_x, tp_y)):
            part = toks.at[src, own_half, pl.ds(n * cut_rows, cut_rows)]
            sides[k].append(
                go(remote(part, part, side_send.at[k, n], side_recv.at[k, n], place(me, column)))
            )
        piece = toks.at[src, own_half]
        pairs[k] = go(
            remote(piece, piece, pair_send.at[2 * k], pair_recv.at[2 * k], place(mate, tp))
        )

    def spread_side(k):
        src = partner(k) * 2 + core
        for copy in sides[k]:
            copy.wait_recv()
        piece = toks.at[src, 1 - own_half]
        half_pairs[k] = go(
            remote(piece, piece, pair_send.at[2 * k + 1], pair_recv.at[2 * k + 1], place(mate, tp))
        )

    def settle(k):
        pairs[k].wait_recv()
        half_pairs[k].wait_recv()

    def chosen(source):
        slots = meta_in[source]
        at = lax.broadcasted_iota(jnp.int32, (capacity, tok_rows), 0).astype(jnp.float32)
        hits = [at == slots[n : n + 1, :] for n in range(local_count)]
        ones = jnp.concatenate([h.astype(jnp.float32) for h in hits], axis=0)
        scale = jnp.concatenate(
            [
                jnp.sum(
                    jnp.where(hits[n], slots[local_count + n : local_count + n + 1, :], 0.0),
                    axis=1,
                    keepdims=True,
                )
                for n in range(local_count)
            ],
            axis=0,
        )
        return ones.astype(jnp.bfloat16), scale

    halves = toks.shape[1]
    width = toks.shape[3]

    def first_half(k):
        s = partner(k)

        @pl.loop(0, 2)
        def _(j):
            ones, _ = chosen(2 * s + j)
            for h in range(halves):
                got = jnp.dot(ones, toks[2 * s + j, h], preferred_element_type=jnp.float32)
                got = got.astype(jnp.bfloat16)
                for n in range(local_count):
                    rows[n, j, :, h * width : (h + 1) * width] = got[
                        n * capacity : (n + 1) * capacity
                    ]

        @pl.loop(0, local_count)
        def _(n):
            block = rows[n].reshape(2 * capacity, halves * width)
            cut = units // 2
            for part in range(2):
                cols = slice(part * cut, (part + 1) * cut)
                gate = jnp.dot(block, gate_w[n, :, cols], preferred_element_type=jnp.float32)
                up = jnp.dot(block, up_w[n, :, cols], preferred_element_type=jnp.float32)
                acts[k, tp, n, :, cols] = clamped_units(gate, up).astype(jnp.bfloat16)

    own_x, own_y, fwd_y, fwd_x = {}, {}, {}, {}

    def send_act(k):
        piece = acts.at[k, tp]
        own_x[k] = go(
            remote(piece, piece, act_send.at[k, 0], act_recv.at[k, 0], place(me, tp_x))
        )
        own_y[k] = go(
            remote(piece, piece, act_send.at[k, 1], act_recv.at[k, 1], place(me, tp_y))
        )

    def forward_act(k):
        mid = local_count // 2
        own_x[k].wait_recv()
        piece = acts.at[k, tp_x, pl.ds(0, mid)]
        fwd_y[k] = go(
            remote(piece, piece, act_send.at[k, 2], act_recv.at[k, 2], place(me, tp_y))
        )
        own_y[k].wait_recv()
        piece = acts.at[k, tp_y, pl.ds(mid, local_count - mid)]
        fwd_x[k] = go(
            remote(piece, piece, act_send.at[k, 3], act_recv.at[k, 3], place(me, tp_x))
        )

    sums = {}

    def second_half(k):
        s = partner(k)
        fwd_y[k].wait_recv()
        fwd_x[k].wait_recv()

        @pl.loop(0, local_count)
        def _(n):
            total = jnp.zeros((2 * capacity, down_w.shape[2]), jnp.float32)
            for t in range(acts.shape[1]):
                total = total + jnp.dot(
                    acts[k, t, n],
                    down_w[n, t * units : (t + 1) * units, :],
                    preferred_element_type=jnp.float32,
                )
            weighted[n] = total.reshape(2, capacity, down_w.shape[2])

        def combined(j):
            ones, scale = chosen(2 * s + j)
            value = jnp.concatenate([weighted[n, j] for n in range(local_count)], axis=0)
            value = (value * scale).astype(jnp.bfloat16)
            return lax.dot_general(
                ones, value, (((0,), (0,)), ((), ())), preferred_element_type=jnp.float32
            )

        pair_out[k] = combined(1 - core).astype(jnp.bfloat16)
        sums[k] = go(
            remote(pair_out.at[k], pair_in.at[k], sum_send.at[k], sum_recv.at[k], place(mate, tp))
        )
        mine = combined(core)
        sums[k].wait_recv()
        both = mine + pair_in[k].astype(jnp.float32)
        if k == 0:
            total_ref[...] = both
        else:
            back_out[k] = both.astype(jnp.bfloat16)
            go(
                remote(
                    back_out.at[k],
                    back_in.at[z],
                    back_send.at[k],
                    back_recv.at[z],
                    place(s * 2 + core, tp),
                )
            )


    own_meta.wait()
    for copy in metas:
        copy.wait_recv()
    own_tok.wait()
    own_pair.wait_recv()
    loads[0].wait()
    loads[1].wait()
    first_half(0)
    send_act(0)
    loads[2].wait()
    spread_line(1)
    forward_act(0)
    if chips > 2:
        spread_line(2)
    for k in range(1, chips):
        spread_side(k)
        settle(k)
        first_half(k)
        send_act(k)
        if k + 2 < chips:
            spread_line(k + 2)
        second_half(k - 1)
        forward_act(k)
    second_half(chips - 1)
    result = total_ref[...]
    for k in range(1, chips):
        other = (z + k) % chips
        remote(
            back_out.at[k], back_in.at[other], back_send.at[k], back_recv.at[other], place(mate, tp)
        ).wait_recv()
        result = result + back_in[other].astype(jnp.float32)
    out_ref[...] = result.astype(out_ref.dtype)
    for copy in pending:
        copy.wait_send()

    @pl.when(z < chips - 1)
    def _():
        line(z, 1, None).wait_send()

    @pl.when(z > 0)
    def _():
        line(z, 0, None).wait_send()

    for k in range(1, chips):
        chip = partner(k)

        @pl.when(goes_on(chip))
        def _():
            line(chip, upward(chip), k).wait_send()


def fused_per_device(tokens, norm_gain, route_ids, route_weights, w_gate, w_up, w_down):
    local_count, width, units = w_gate.shape
    out_cols = w_down.shape[2]
    sources = lax.axis_size("ep")
    tp_count = lax.axis_size("tp")
    experts = local_count * sources
    tok_rows, top_count = route_ids.shape
    capacity = 3 * tok_rows * top_count // (2 * experts)
    chips = sources // 2
    half = width // 2
    hits = route_ids[:, :, None] == jnp.arange(experts, dtype=jnp.int32)[None, None, :]
    named = jnp.any(hits, axis=1)
    weight_of = jnp.sum(jnp.where(hits, route_weights[:, :, None], 0.0), axis=1)
    order = jnp.arange(tok_rows)
    before = (order[:, None] > order[None, :]).astype(jnp.bfloat16)
    slot = jnp.dot(before, named.astype(jnp.bfloat16), preferred_element_type=jnp.float32)
    slot = jnp.where(named, slot, -1.0)
    pad = (-2 * local_count) % 8
    meta = jnp.concatenate(
        [
            slot.T.reshape(sources, local_count, tok_rows),
            weight_of.T.reshape(sources, local_count, tok_rows),
            jnp.zeros((sources, pad, tok_rows), jnp.float32),
        ],
        axis=1,
    )
    dma = pltpu.SemaphoreType.DMA
    bf16 = jnp.bfloat16
    vmem = pl.BlockSpec(memory_space=pltpu.VMEM)
    hbm = pl.BlockSpec(memory_space=pltpu.HBM)
    return pl.pallas_call(
        functools.partial(layer_kernel, capacity),
        out_shape=jax.ShapeDtypeStruct((tok_rows, out_cols), bf16),
        in_specs=[vmem, vmem, vmem, hbm, hbm, hbm],
        out_specs=vmem,
        scratch_shapes=[
            pltpu.VMEM(w_gate.shape, bf16),
            pltpu.VMEM(w_up.shape, bf16),
            pltpu.VMEM(w_down.shape, bf16),
            pltpu.VMEM((2, tok_rows, half), bf16),
            pltpu.VMEM((sources, 2, tok_rows, half), bf16),
            pltpu.VMEM(meta.shape, jnp.float32),
            pltpu.VMEM((local_count, 2, capacity, width), bf16),
            pltpu.VMEM((chips, tp_count, local_count, 2 * capacity, units), bf16),
            pltpu.VMEM((local_count, 2, capacity, out_cols), jnp.float32),
            pltpu.VMEM((chips, tok_rows, out_cols), bf16),
            pltpu.VMEM((chips, tok_rows, out_cols), bf16),
            pltpu.VMEM((chips, tok_rows, out_cols), bf16),
            pltpu.VMEM((chips, tok_rows, out_cols), bf16),
            pltpu.VMEM((tok_rows, out_cols), jnp.float32),
            dma((3,)),
            dma((2,)),
            dma((sources,)),
            dma((sources,)),
            dma((2, chips)),
            dma((2, chips)),
            dma((chips, 2)),
            dma((chips, 2)),
            dma((2 * chips,)),
            dma((2 * chips,)),
            dma((chips, 4)),
            dma((chips, 4)),
            dma((chips,)),
            dma((chips,)),
            dma((chips,)),
            dma((chips,)),
        ],
        compiler_params=pltpu.CompilerParams(
            collective_id=0, has_side_effects=True, vmem_limit_bytes=60 * 1024 * 1024
        ),
    )(tokens, norm_gain.reshape(1, width), meta, w_gate, w_up, w_down)


def pick_plan(mesh):
    sources, tp_count = mesh.shape["ep"], mesh.shape["tp"]

    def body(tokens, norm_gain, route_ids, route_weights, w_gate, w_up, w_down):
        tok_rows, top_count = route_ids.shape
        experts = w_gate.shape[0] * sources
        capacity = 3 * tok_rows * top_count // (2 * experts)
        gathered = 2 * tokens.size * sources + 6 * w_gate.size
        fused = (
            tp_count == 4
            and sources in (4, 8)
            and capacity % 16 == 0
            and w_gate.shape[0] % 2 == 0
            and tok_rows % 32 == 0
            and gathered < 32 * 1024 * 1024
        )
        run = fused_per_device if fused else per_device
        return run(tokens, norm_gain, route_ids, route_weights, w_gate, w_up, w_down)

    return body


def solution(mesh):
    return jax.shard_map(
        pick_plan(mesh),
        mesh=mesh,
        in_specs=(
            P("ep", None),
            P(),
            P("ep", None),
            P("ep", None),
            P("ep", None, "tp"),
            P("ep", None, "tp"),
            P("ep", None, "tp"),
        ),
        out_specs=P("ep", "tp"),
        check_vma=False,
    )
```

profile of v0, /device:TPU:1, one launch (start us, length us, event | category | flops | bytes accessed | tf_op | source)
XLA Modules:
  0.0 109.1 jit_solution(4395536117005559076)
XLA Ops:
  0.0 0.1 pad.2.clone
  0.1 0.7 fusion
  0.8 0.2 convolution_select_fusion
  1.0 0.7 select_reduce_fusion
  1.7 0.7 maximum_maximum_fusion.meta_ref
  2.4 105.0 %shard_map.73 = bf16[256,512]{1,0:T(8,128)(2,1)} custom-call(bf16[256,2048]{1,0:T(8,128)(2,1)} %tokens_ref.1, f32[1,2048]{1,0:T(1,128)} %bitcast.6, f32[8,8,256]{2,1,0:T(8,128)} %maximum_maximum_fusion.meta_ref, bf16[2,2048,512]{2,1,0:T(8,128)(2,1)} %gate_hbm.1, bf16[2,2048,512]{2,1,0:T(8,128)(2,1)} %up_hbm.1, bf16[2,2048,512]{2,1,0:T(8,128)(2,1)} %down_hbm.1), custom_call_target="tpu_custom_call" | custom-call | tf_op jit(solution)/shard_map/pallas_call | solution.py:485
  107.4 1.7 %copy.11 = bf16[256,512]{1,0:T(8,128)(2,1)} copy(bf16[256,512]{1,0:T(8,128)(2,1)} %shard_map.73) | data formatting | bytes 524288
  (3 shorter events, 0.1 us)
where the time goes:
time: 110 us; the launch traced here: 109 us
  Pallas kernels  105 us (95%)
  other arithmetic  2.12 us (2%)
  local copies, waits for them, and re-layouts  1.8 us (2%)
    pallas_call x1, Pallas kernels, fused_per_device(): pl.pallas_call(functools.partial(layer_kernel, capacity), out_shape=jax.S...  105 us

commit v1 on v0

v1 whole, which is shorter than its diff:
```python
import functools
import jax
import jax.numpy as jnp
from jax import lax
from jax.experimental import pallas as pl
from jax.experimental.pallas import tpu as pltpu
from jax.sharding import PartitionSpec as P

swiglu_limit = 7.0
swiglu_alpha = 1.702
norm_eps = 1e-05


def clamped_units(gate_pre, up_pre):
    capped = jnp.minimum(gate_pre, swiglu_limit)
    linear = jnp.clip(up_pre, -swiglu_limit, swiglu_limit)
    return capped * jax.nn.sigmoid(swiglu_alpha * capped) * (linear + 1.0)


def expert_work(outgoing, gate_weight, up_weight, down_weight):
    received = lax.all_to_all(outgoing, "ep", split_axis=1, concat_axis=1, tiled=True)
    local_count, sources, capacity, columns = received.shape
    row_count = sources * capacity
    row_block = received.reshape(local_count, row_count, columns)
    shard_piece = lax.all_gather(row_block, "tp", axis=2, tiled=True)
    gate_sum = jnp.einsum(
        "lrd,ldf->lrf", shard_piece, gate_weight, preferred_element_type=jnp.float32
    )
    up_sum = jnp.einsum("lrd,ldf->lrf", shard_piece, up_weight, preferred_element_type=jnp.float32)
    activation = clamped_units(gate_sum, up_sum).astype(jnp.bfloat16)
    out_cols = down_weight.shape[2]
    result = jnp.einsum(
        "lrf,lfd->lrd",
        lax.all_gather(activation, "tp", axis=2, tiled=True),
        down_weight,
        preferred_element_type=jnp.float32,
    )
    result = result.astype(jnp.bfloat16).reshape(local_count, sources, capacity, out_cols)
    return lax.all_to_all(result, "ep", split_axis=1, concat_axis=1, tiled=True)


def per_device(tokens, norm_gain, route_ids, route_weights, w_gate, w_up, w_down):
    local_count = w_gate.shape[0]
    sources = lax.axis_size("ep")
    tp_count = lax.axis_size("tp")
    width = tokens.shape[1]
    columns = width // tp_count
    experts = local_count * sources
    tok_rows, top_count = route_ids.shape
    capacity = 3 * tok_rows * top_count // (2 * experts)
    values = tokens.astype(jnp.float32)
    row_mean = jnp.mean(values, axis=1, keepdims=True)
    centred = values - row_mean
    row_var = jnp.mean(centred * centred, axis=1, keepdims=True)
    offset = lax.axis_index("tp") * columns
    own_cols = lax.dynamic_slice_in_dim(centred, offset, columns, 1)
    own_gain = lax.dynamic_slice_in_dim(norm_gain, offset, columns, 0)
    normed = (own_cols * lax.rsqrt(row_var + norm_eps) * own_gain).astype(jnp.bfloat16)
    flat_ids = route_ids.reshape(-1)
    matches = (flat_ids[:, None] == jnp.arange(experts, dtype=jnp.int32)[None, :]).astype(jnp.int32)
    earlier = jnp.cumsum(matches, axis=0) - matches
    slot_index = jnp.sum(earlier * matches, axis=1)
    position = (
        flat_ids % local_count * (sources * capacity)
        + flat_ids // local_count * capacity
        + slot_index
    )
    buffer_rows = local_count * sources * capacity
    placed = (
        position.reshape(tok_rows, top_count)[:, :, None]
        == jnp.arange(buffer_rows, dtype=jnp.int32)[None, None, :]
    )
    placement_matrix = jnp.any(placed, axis=1).astype(jnp.bfloat16)
    outgoing = jnp.einsum("tp,td->pd", placement_matrix, normed, preferred_element_type=jnp.float32)
    outgoing = outgoing.astype(jnp.bfloat16).reshape(local_count, sources, capacity, columns)
    returned = jnp.concatenate(
        [
            expert_work(
                outgoing[number : number + 1],
                w_gate[number : number + 1],
                w_up[number : number + 1],
                w_down[number : number + 1],
            )
            for number in range(local_count)
        ],
        axis=0,
    )
    flat_out = returned.reshape(buffer_rows, columns)
    picked = flat_out[position].reshape(tok_rows, top_count, columns).astype(jnp.float32)
    return jnp.sum(picked * route_weights[:, :, None], axis=1).astype(jnp.bfloat16)


CUT_EIGHTHS = 6
STAGES = (
    ("F", 1),
    ("L", 1, 0, 0),
    ("W", 1),
    ("L", 1, 0, 1),
    ("L", 1, 1, 0),
    ("S", 1, 0),
    ("L", 1, 1, 1),
    ("W", 0),
    ("F", 2),
    ("S", 1, 1),
    ("F", 3),
    ("W", 2),
    ("L", 2, 1, 0),
    ("L", 2, 1, 1),
    ("W", 3),
    ("S", 2, 1),
    ("L", 2, 0, 0),
    ("D", 2),
    ("L", 3, 1, 1),
    ("L", 3, 1, 0),
    ("F", 5),
    ("L", 3, 0, 0),
    ("S", 3, 1),
    ("R", 2),
    ("L", 2, 0, 1),
    ("D", 3),
    ("F", 7),
    ("D", 0),
    ("W", 5),
    ("L", 3, 0, 1),
    ("S", 3, 0),
    ("W", 7),
    ("F", 6),
    ("S", 2, 0),
    ("D", 5),
    ("F", 4),
    ("R", 5),
    ("D", 7),
    ("R", 7),
    ("W", 6),
    ("R", 3),
    ("W", 4),
    ("D", 6),
    ("R", 6),
    ("D", 4),
    ("D", 1),
    ("R", 4),
    ("R", 1),
)


def layer_kernel(
    capacity,
    tokens_hbm,
    gain_hbm,
    ids_hbm,
    mix_hbm,
    gate_hbm,
    up_hbm,
    down_hbm,
    out_ref,
    gate_w,
    up_w,
    down_w,
    tok_in,
    gain_in,
    ids_in,
    mix_in,
    toks,
    meta,
    earlier,
    rows,
    acts,
    weighted,
    combined,
    pair_out,
    pair_in,
    back_out,
    back_in,
    weight_sem,
    tok_sem,
    local_sem,
    meta_send,
    meta_recv,
    own_send,
    own_recv,
    line_send,
    line_recv,
    side_send,
    side_recv,
    mate_send,
    mate_recv,
    act_send,
    act_recv,
    pair_send,
    pair_recv,
    back_send,
    back_recv,
):
    sources = toks.shape[0]
    chips = sources // 2
    local_count = gate_w.shape[0]
    units = gate_w.shape[2]
    tok_rows = tok_in.shape[0]
    quarter = toks.shape[4]
    out_cols = down_w.shape[2]
    half_rows = tok_rows // 2
    cut = tok_rows * CUT_EIGHTHS // 8
    me = lax.axis_index("ep")
    tp = lax.axis_index("tp")
    z, core = me // 2, me % 2
    y, x = tp // 2, tp % 2
    tp_x = y * 2 + (1 - x)
    tp_y = (1 - y) * 2 + x
    side_tp = tp_x * (1 - core) + tp_y * core
    mate = z * 2 + (1 - core)
    own_half = (x + y) % 2
    parts = 2 if cut < tok_rows else 1

    def partner(k):
        chosen_chip = 0 * z
        for at in range(chips):
            sign = 1 if 2 * at < chips else -1
            order = sorted(range(chips), key=lambda c: (abs(c - at), sign * c))
            gap = (z - at) * (z - at)
            chosen_chip = chosen_chip + order[k] * (1 - (gap + chips * chips - 1) // (chips * chips))
        return chosen_chip

    def place(ep, column):
        return {"ep": ep, "tp": column}

    def remote(source, target, send, recv, where):
        return pltpu.make_async_remote_copy(
            src_ref=source,
            dst_ref=target,
            send_sem=send,
            recv_sem=recv,
            device_id=where,
            device_id_type=pl.DeviceIdType.MESH,
        )

    barrier = pltpu.get_barrier_semaphore()
    for d in range(1, sources):
        pl.semaphore_signal(
            barrier, inc=1, device_id=place((me + d) % sources, tp), device_id_type=pl.DeviceIdType.MESH
        )
    for column in (tp_x, tp_y):
        pl.semaphore_signal(
            barrier, inc=1, device_id=place(me, column), device_id_type=pl.DeviceIdType.MESH
        )

    piece_count = tok_sem.shape[0]
    piece_rows = tok_rows // piece_count
    tok_loads = [
        pltpu.make_async_copy(
            tokens_hbm.at[pl.ds(n * piece_rows, piece_rows)],
            tok_in.at[pl.ds(n * piece_rows, piece_rows)],
            tok_sem.at[n],
        )
        for n in range(piece_count)
    ]
    small = [
        pltpu.make_async_copy(gain_hbm, gain_in, local_sem.at[0]),
        pltpu.make_async_copy(ids_hbm, ids_in.at[me], local_sem.at[1]),
        pltpu.make_async_copy(mix_hbm, mix_in.at[me], local_sem.at[2]),
    ]
    loads = [
        pltpu.make_async_copy(hbm, vmem, weight_sem.at[n])
        for n, (hbm, vmem) in enumerate(((gate_hbm, gate_w), (up_hbm, up_w), (down_hbm, down_w)))
    ]
    for copy in small + tok_loads + loads:
        copy.start()

    before = lax.broadcasted_iota(jnp.int32, (tok_rows, tok_rows), 0)
    after = lax.broadcasted_iota(jnp.int32, (tok_rows, tok_rows), 1)
    earlier[...] = (before < after).astype(jnp.float32).astype(jnp.bfloat16)

    def make_meta(source):
        ids, mix = ids_in[source], mix_in[source]
        named, scales = [], []
        for n in range(local_count):
            match = ids == me * local_count + n
            named.append(jnp.sum(match.astype(jnp.float32), axis=0, keepdims=True))
            scales.append(jnp.sum(jnp.where(match, mix, 0.0), axis=0, keepdims=True))
        pad = [jnp.zeros((1, tok_rows), jnp.float32)] * (8 - local_count)
        names = jnp.concatenate(named + pad, axis=0)
        slot = jnp.dot(names.astype(jnp.bfloat16), earlier[...], preferred_element_type=jnp.float32)
        slot = jnp.where(names > 0.0, slot, -1.0)
        meta[source, 0] = slot
        meta[source, 1] = jnp.concatenate(scales + pad, axis=0)

    for copy in small:
        copy.wait()
    band = 32

    @pl.loop(0, piece_count)
    def _(p):
        pltpu.make_async_copy(
            tokens_hbm.at[pl.ds(0, piece_rows)], tok_in.at[pl.ds(0, piece_rows)], tok_sem.at[p]
        ).wait()
        for n in range(piece_rows // band):
            at = pl.ds(pl.multiple_of(p * piece_rows + n * band, band), band)
            values = tok_in[at, :].astype(jnp.float32)
            centred = values - jnp.mean(values, axis=1, keepdims=True)
            row_var = jnp.mean(centred * centred, axis=1, keepdims=True)
            normal = (centred * lax.rsqrt(row_var + norm_eps) * gain_in[...]).astype(jnp.bfloat16)
            for q in range(4):
                toks[me, q // 2, q % 2, at, :] = normal[:, q * quarter : (q + 1) * quarter]

    pending = []

    def go(copy):
        copy.start()
        pending.append(copy)
        return copy

    def always(condition, copy):
        pending.append((condition, copy))

    def line(chip, i, e, up):
        source = chip * 2 + i
        if e == 0:
            piece = toks.at[source, own_half, core]
        else:
            piece = toks.at[source, 1 - own_half, core, pl.ds(cut, tok_rows - cut)]
        return remote(
            piece,
            piece,
            line_send.at[up, chip, i, e],
            line_recv.at[chip, i, e],
            place((z + 2 * up - 1) * 2 + core, tp),
        )

    def side(chip, i):
        piece = toks.at[chip * 2 + i, own_half, core, pl.ds(0, cut)]
        return remote(
            piece, piece, side_send.at[chip, i], side_recv.at[chip, i], place(me, side_tp)
        )

    def to_mate(chip, i, m):
        source = chip * 2 + i
        piece = (
            toks.at[source, own_half, core],
            toks.at[source, 1 - own_half, core, pl.ds(cut, tok_rows - cut)] if parts > 1 else None,
            toks.at[source, 1 - own_half, core, pl.ds(0, cut)],
        )[m]
        return remote(
            piece, piece, mate_send.at[chip, i, m], mate_recv.at[chip, i, m], place(mate, tp)
        )

    mate_parts = (0, 1, 2) if parts > 1 else (0, 2)
    ends = ((1, z < chips - 1), (0, z > 0))

    def start_line(i):
        for e in range(parts):
            for up, there in ends:

                @pl.when(there)
                def _():
                    line(z, i, e, up).start()

    own_pieces = (
        toks.at[me, own_half, 1 - core],
        toks.at[me, 1 - own_half, 1 - core],
        toks.at[me, :, core],
    )
    own_copies = []
    metas = []
    acts_sent = {}

    def run_start():
        pl.semaphore_wait(barrier, sources + 1)
        for n, piece in enumerate(own_pieces):
            own_copies.append(
                go(remote(piece, piece, own_send.at[n], own_recv.at[n], place(mate, tp)))
            )

        @pl.when(core == 0)
        def _():
            start_line(0)

        send_act(0)
        for d in range(1, sources):
            for n, table in enumerate((ids_in, mix_in)):
                metas.append(
                    go(
                        remote(
                            table.at[me],
                            table.at[me],
                            meta_send.at[n, d],
                            meta_recv.at[n, d],
                            place((me + d) % sources, tp),
                        )
                    )
                )
        own_copies[0].wait_recv()
        own_copies[1].wait_recv()

        @pl.when(core == 1)
        def _():
            start_line(0)

        start_line(1)
        for up, there in ends:
            for i in range(2):
                for e in range(parts):
                    always(there, line(z, i, e, up))
        for copy in metas:
            copy.wait_recv()

        @pl.loop(1, sources)
        def _(d):
            make_meta((me + d) % sources)

    def run_line(distance, i, e):
        for up, chip in ((1, z - distance), (0, z + distance)):
            here = chip >= 0 if up else chip < chips
            ahead = z + 2 * up - 1
            onward = jnp.logical_and(here, ahead < chips if up else ahead >= 0)

            @pl.when(here)
            def _():
                line(chip, i, e, up).wait_recv()

                @pl.when(ahead < chips if up else ahead >= 0)
                def _():
                    line(chip, i, e, up).start()

                if e == 0:
                    side(chip, i).start()
                to_mate(chip, i, e).start()

            always(onward, line(chip, i, e, up))
            if e == 0:
                always(here, side(chip, i))
            always(here, to_mate(chip, i, e))

    def run_side(k, i):
        chip = partner(k)
        side(chip, i).wait_recv()
        go(to_mate(chip, i, 2))

    def chosen(source):
        slots, scales = meta[source, 0], meta[source, 1]
        at = lax.broadcasted_iota(jnp.int32, (capacity, tok_rows), 0).astype(jnp.float32)
        hits = [at == slots[n : n + 1, :] for n in range(local_count)]
        ones = jnp.concatenate([h.astype(jnp.float32) for h in hits], axis=0)
        scale = jnp.concatenate(
            [
                jnp.sum(jnp.where(hits[n], scales[n : n + 1, :], 0.0), axis=1, keepdims=True)
                for n in range(local_count)
            ],
            axis=0,
        )
        return ones.astype(jnp.bfloat16), scale

    def source_of(s):
        if s == 0:
            return me
        if s == 1:
            return mate
        return partner(s // 2) * 2 + s % 2

    def compute_act(s):
        source = source_of(s)
        ones, _ = chosen(source)
        for q in range(4):
            got = jnp.dot(ones, toks[source, q // 2, q % 2], preferred_element_type=jnp.float32)
            got = got.astype(jnp.bfloat16)
            for n in range(local_count):
                rows[n, :, q * quarter : (q + 1) * quarter] = got[n * capacity : (n + 1) * capacity]

        @pl.loop(0, local_count)
        def _(n):
            block = rows[n]
            half = units // 2
            for part in range(2):
                cols = slice(part * half, (part + 1) * half)
                gate = jnp.dot(block, gate_w[n, :, cols], preferred_element_type=jnp.float32)
                up = jnp.dot(block, up_w[n, :, cols], preferred_element_type=jnp.float32)
                acts[s, tp, n, :, cols] = clamped_units(gate, up).astype(jnp.bfloat16)

    def send_act(s):
        piece = acts.at[s, tp]
        acts_sent[s] = [
            go(remote(piece, piece, act_send.at[s, n], act_recv.at[s, n], place(me, column)))
            for n, column in enumerate((tp_x, tp_y))
        ]

    def run_first(s):
        if s == 1:
            own_copies[2].wait_recv()
        elif s > 1:
            chip = partner(s // 2)
            for m in mate_parts:
                to_mate(chip, s % 2, m).wait_recv()
        compute_act(s)
        send_act(s)

    def run_forward(s):
        mid = local_count // 2
        for n, (origin, column, at, size) in enumerate(
            ((tp_x, tp_y, 0, mid), (tp_y, tp_x, mid, local_count - mid))
        ):
            acts_sent[s][n].wait_recv()
            piece = acts.at[s, origin, pl.ds(at, size)]
            acts_sent[s].append(
                go(
                    remote(
                        piece, piece, act_send.at[s, 2 + n], act_recv.at[s, 2 + n], place(me, column)
                    )
                )
            )

    pairs = {}

    def run_second(s):
        acts_sent[s][2].wait_recv()
        acts_sent[s][3].wait_recv()

        @pl.loop(0, local_count)
        def _(n):
            total = jnp.zeros((capacity, out_cols), jnp.float32)
            for t in range(acts.shape[1]):
                total = total + jnp.dot(
                    acts[s, t, n],
                    down_w[n, t * units : (t + 1) * units, :],
                    preferred_element_type=jnp.float32,
                )
            weighted[n] = total

        ones, scale = chosen(source_of(s))
        value = jnp.concatenate([weighted[n] for n in range(local_count)], axis=0)
        value = (value * scale).astype(jnp.bfloat16)
        result = lax.dot_general(
            ones, value, (((0,), (0,)), ((), ())), preferred_element_type=jnp.float32
        )
        for h in range(2):
            combined[s, h] = result[h * half_rows : (h + 1) * half_rows]
        if s == 1:
            for h in range(2):
                pair_out[0, h] = combined[1, h].astype(jnp.bfloat16)
            piece, target = pair_out.at[0], pair_in.at[0]
        elif s > 1:
            pair_out[s // 2, s % 2] = combined[s, 1 - core].astype(jnp.bfloat16)
            piece, target = pair_out.at[s // 2, s % 2], pair_in.at[s // 2, s % 2]
        if s > 0:
            pairs[s] = go(remote(piece, target, pair_send.at[s], pair_recv.at[s], place(mate, tp)))

    def run_back(s):
        pairs[s].wait_recv()
        if s > 1:
            k, i = s // 2, s % 2
            both = combined[s, core] + pair_in[k, i].astype(jnp.float32)
            back_out[k, i] = both.astype(jnp.bfloat16)
            go(
                remote(
                    back_out.at[k, i],
                    back_in.at[z, core],
                    back_send.at[k, i],
                    back_recv.at[z, core],
                    place(partner(k) * 2 + i, tp),
                )
            )

    make_meta(me)
    loads[0].wait()
    loads[1].wait()
    compute_act(0)
    run_start()
    loads[2].wait()
    runs = {
        "L": run_line,
        "S": run_side,
        "F": run_first,
        "W": run_forward,
        "D": run_second,
        "R": run_back,
    }
    for kind, *rest in STAGES:
        runs[kind](*rest)
    for h in range(2):
        result = combined[0, h] + pair_in[0, h].astype(jnp.float32)
        for d in range(1, chips):
            chip = (z + d) % chips
            remote(
                back_out.at[0, 0], back_in.at[chip, h], back_send.at[0, h], back_recv.at[chip, h], place(mate, tp)
            ).wait_recv()
            result = result + back_in[chip, h].astype(jnp.float32)
        out_ref[h * half_rows : (h + 1) * half_rows, :] = result.astype(out_ref.dtype)
    for entry in pending:
        if isinstance(entry, tuple):

            @pl.when(entry[0])
            def _():
                entry[1].wait_send()
        else:
            entry.wait_send()


def fused_per_device(tokens, norm_gain, route_ids, route_weights, w_gate, w_up, w_down):
    local_count, width, units = w_gate.shape
    out_cols = w_down.shape[2]
    sources = lax.axis_size("ep")
    tp_count = lax.axis_size("tp")
    experts = local_count * sources
    tok_rows, top_count = route_ids.shape
    capacity = 3 * tok_rows * top_count // (2 * experts)
    chips = sources // 2
    quarter = width // 4
    half_rows = tok_rows // 2
    dma = pltpu.SemaphoreType.DMA
    bf16 = jnp.bfloat16
    vmem = pl.BlockSpec(memory_space=pltpu.VMEM)
    hbm = pl.BlockSpec(memory_space=pltpu.HBM)
    return pl.pallas_call(
        functools.partial(layer_kernel, capacity),
        out_shape=jax.ShapeDtypeStruct((tok_rows, out_cols), bf16),
        in_specs=[hbm] * 7,
        out_specs=vmem,
        scratch_shapes=[
            pltpu.VMEM(w_gate.shape, bf16),
            pltpu.VMEM(w_up.shape, bf16),
            pltpu.VMEM(w_down.shape, bf16),
            pltpu.VMEM(tokens.shape, bf16),
            pltpu.VMEM((1, width), jnp.float32),
            pltpu.VMEM((sources, top_count, tok_rows), jnp.int32),
            pltpu.VMEM((sources, top_count, tok_rows), jnp.float32),
            pltpu.VMEM((sources, 2, 2, tok_rows, quarter), bf16),
            pltpu.VMEM((sources, 2, 8, tok_rows), jnp.float32),
            pltpu.VMEM((tok_rows, tok_rows), bf16),
            pltpu.VMEM((local_count, capacity, width), bf16),
            pltpu.VMEM((sources, tp_count, local_count, capacity, units), bf16),
            pltpu.VMEM((local_count, capacity, out_cols), jnp.float32),
            pltpu.VMEM((sources, 2, half_rows, out_cols), jnp.float32),
            pltpu.VMEM((chips, 2, half_rows, out_cols), bf16),
            pltpu.VMEM((chips, 2, half_rows, out_cols), bf16),
            pltpu.VMEM((chips, 2, half_rows, out_cols), bf16),
            pltpu.VMEM((chips, 2, half_rows, out_cols), bf16),
            dma((3,)),
            dma((4,)),
            dma((3,)),
            dma((2, sources)),
            dma((2, sources)),
            dma((3,)),
            dma((3,)),
            dma((2, chips, 2, 2)),
            dma((chips, 2, 2)),
            dma((chips, 2)),
            dma((chips, 2)),
            dma((chips, 2, 3)),
            dma((chips, 2, 3)),
            dma((sources, 4)),
            dma((sources, 4)),
            dma((sources,)),
            dma((sources,)),
            dma((chips, 2)),
            dma((chips, 2)),
        ],
        compiler_params=pltpu.CompilerParams(
            collective_id=0, has_side_effects=True, vmem_limit_bytes=60 * 1024 * 1024
        ),
    )(tokens, norm_gain.reshape(1, width), route_ids.T, route_weights.T, w_gate, w_up, w_down)


def pick_plan(mesh):
    sources, tp_count = mesh.shape["ep"], mesh.shape["tp"]

    def body(tokens, norm_gain, route_ids, route_weights, w_gate, w_up, w_down):
        tok_rows, top_count = route_ids.shape
        experts = w_gate.shape[0] * sources
        capacity = 3 * tok_rows * top_count // (2 * experts)
        gathered = 2 * tokens.size * sources + 6 * w_gate.size
        fused = (
            tp_count == 4
            and sources == 8
            and capacity % 16 == 0
            and w_gate.shape[0] in (2, 4, 6, 8)
            and tok_rows % 128 == 0
            and tokens.shape[1] % 512 == 0
            and gathered < 32 * 1024 * 1024
        )
        run = fused_per_device if fused else per_device
        return run(tokens, norm_gain, route_ids, route_weights, w_gate, w_up, w_down)

    return body


def solution(mesh):
    return jax.shard_map(
        pick_plan(mesh),
        mesh=mesh,
        in_specs=(
            P("ep", None),
            P(),
            P("ep", None),
            P("ep", None),
            P("ep", None, "tp"),
            P("ep", None, "tp"),
            P("ep", None, "tp"),
        ),
        out_specs=P("ep", "tp"),
        check_vma=False,
    )
```

time: 110 us -> 103 us (0.936)
  the two profiles are of different devices: /device:TPU:1 before, /device:TPU:8 now
where the time goes in v1:
time: 103 us
  Pallas kernels  101 us (98%)
  local copies, waits for them, and re-layouts  1.67 us (2%)
    pallas_call x1, Pallas kernels, fused_per_device(): pl.pallas_call(functools.partial(layer_kernel, capacity), out_shape=jax.S...  101 us

profile of v1, /device:TPU:8, one launch (start us, length us, event | category | flops | bytes accessed | tf_op | source)
XLA Modules:
  0.0 102.5 jit_solution(2259031336110081156)
XLA Ops:
  0.0 100.8 %shard_map.73 = bf16[256,512]{1,0:T(8,128)(2,1)} custom-call(bf16[256,2048]{1,0:T(8,128)(2,1)} %tokens_hbm.1, f32[1,2048]{1,0:T(1,128)} %bitcast.3, s32[4,256]{1,0:T(4,128)} %bitcast.4, f32[4,256]{1,0:T(4,128)} %bitcast.5, bf16[2,2048,512]{2,1,0:T(8,128)(2,1)} %gate_hbm.1, bf16[2,2048,512]{2,1,0:T(8,128)(2,1)} %up_hbm.1, bf16[2,2048,512]{2,1,0:T(8,128)(2,1)} %down_hbm.1), custom_call_target="tpu_custom_call" | custom-call | tf_op jit(solution)/shard_map/pallas_call | solution.py:610
  100.8 1.7 %copy.9 = bf16[256,512]{1,0:T(8,128)(2,1)} copy(bf16[256,512]{1,0:T(8,128)(2,1)} %shard_map.73) | data formatting | bytes 524288

commit v2 on v1

--- a/solution.py
+++ b/solution.py
@@ -92,53 +92,53 @@
 
 CUT_EIGHTHS = 6
 STAGES = (
+    ("L", 1, 0, 0),
     ("F", 1),
-    ("L", 1, 0, 0),
-    ("W", 1),
     ("L", 1, 0, 1),
-    ("L", 1, 1, 0),
     ("S", 1, 0),
-    ("L", 1, 1, 1),
     ("W", 0),
     ("F", 2),
+    ("L", 1, 1, 1),
+    ("L", 1, 1, 0),
+    ("L", 2, 0, 0),
+    ("W", 2),
+    ("L", 2, 1, 1),
+    ("L", 2, 0, 1),
+    ("S", 2, 0),
+    ("L", 2, 1, 0),
+    ("F", 4),
+    ("S", 2, 1),
     ("S", 1, 1),
+    ("L", 3, 0, 0),
+    ("F", 5),
+    ("W", 4),
     ("F", 3),
-    ("W", 2),
-    ("L", 2, 1, 0),
-    ("L", 2, 1, 1),
-    ("W", 3),
-    ("S", 2, 1),
-    ("L", 2, 0, 0),
+    ("D", 0),
+    ("L", 3, 0, 1),
+    ("L", 3, 1, 0),
+    ("W", 5),
+    ("S", 3, 0),
+    ("L", 3, 1, 1),
+    ("F", 6),
+    ("D", 4),
     ("D", 2),
-    ("L", 3, 1, 1),
-    ("L", 3, 1, 0),
-    ("F", 5),
-    ("L", 3, 0, 0),
     ("S", 3, 1),
     ("R", 2),
-    ("L", 2, 0, 1),
+    ("R", 4),
+    ("W", 3),
+    ("D", 5),
+    ("W", 6),
+    ("F", 7),
+    ("R", 5),
     ("D", 3),
-    ("F", 7),
-    ("D", 0),
-    ("W", 5),
-    ("L", 3, 0, 1),
-    ("S", 3, 0),
+    ("D", 6),
+    ("R", 3),
     ("W", 7),
-    ("F", 6),
-    ("S", 2, 0),
-    ("D", 5),
-    ("F", 4),
-    ("R", 5),
+    ("W", 1),
+    ("R", 6),
     ("D", 7),
     ("R", 7),
-    ("W", 6),
-    ("R", 3),
-    ("W", 4),
-    ("D", 6),
-    ("R", 6),
-    ("D", 4),
     ("D", 1),
-    ("R", 4),
     ("R", 1),
 )
 
@@ -262,7 +262,7 @@
         pltpu.make_async_copy(hbm, vmem, weight_sem.at[n])
         for n, (hbm, vmem) in enumerate(((gate_hbm, gate_w), (up_hbm, up_w), (down_hbm, down_w)))
     ]
-    for copy in small + tok_loads + loads:
+    for copy in small + tok_loads:
         copy.start()
 
     before = lax.broadcasted_iota(jnp.int32, (tok_rows, tok_rows), 0)
@@ -283,15 +283,14 @@
         meta[source, 0] = slot
         meta[source, 1] = jnp.concatenate(scales + pad, axis=0)
 
-    for copy in small:
+    for copy in small + tok_loads:
         copy.wait()
+    for copy in loads:
+        copy.start()
     band = 32
 
     @pl.loop(0, piece_count)
     def _(p):
-        pltpu.make_async_copy(
-            tokens_hbm.at[pl.ds(0, piece_rows)], tok_in.at[pl.ds(0, piece_rows)], tok_sem.at[p]
-        ).wait()
         for n in range(piece_rows // band):
             at = pl.ds(pl.multiple_of(p * piece_rows + n * band, band), band)
             values = tok_in[at, :].astype(jnp.float32)
@@ -364,16 +363,6 @@
 
     def run_start():
         pl.semaphore_wait(barrier, sources + 1)
-        for n, piece in enumerate(own_pieces):
-            own_copies.append(
-                go(remote(piece, piece, own_send.at[n], own_recv.at[n], place(mate, tp)))
-            )
-
-        @pl.when(core == 0)
-        def _():
-            start_line(0)
-
-        send_act(0)
         for d in range(1, sources):
             for n, table in enumerate((ids_in, mix_in)):
                 metas.append(
@@ -387,6 +376,15 @@
                         )
                     )
                 )
+        for n, piece in enumerate(own_pieces):
+            own_copies.append(
+                go(remote(piece, piece, own_send.at[n], own_recv.at[n], place(mate, tp)))
+            )
+
+        @pl.when(core == 0)
+        def _():
+            start_line(0)
+
         own_copies[0].wait_recv()
         own_copies[1].wait_recv()
 
@@ -399,13 +397,6 @@
             for i in range(2):
                 for e in range(parts):
                     always(there, line(z, i, e, up))
-        for copy in metas:
-            copy.wait_recv()
-
-        @pl.loop(1, sources)
-        def _(d):
-            make_meta((me + d) % sources)
-
     def run_line(distance, i, e):
         for up, chip in ((1, z - distance), (0, z + distance)):
             here = chip >= 0 if up else chip < chips
@@ -482,6 +473,9 @@
         ]
 
     def run_first(s):
+        while metas:
+            metas.pop().wait_recv()
+        make_meta(source_of(s))
         if s == 1:
             own_copies[2].wait_recv()
         elif s > 1:
@@ -557,11 +551,12 @@
                 )
             )
 
+    run_start()
     make_meta(me)
     loads[0].wait()
     loads[1].wait()
     compute_act(0)
-    run_start()
+    send_act(0)
     loads[2].wait()
     runs = {
         "L": run_line,

time: 103 us -> 93.1 us (0.904)
  the two profiles are of different devices: /device:TPU:8 before, /device:TPU:1 now
where the time goes in v2:
time: 93.1 us; the launch traced here: 93 us
  Pallas kernels  91.3 us (98%)
  local copies, waits for them, and re-layouts  1.67 us (2%)
    pallas_call x1, Pallas kernels, fused_per_device(): pl.pallas_call(functools.partial(layer_kernel, capacity), out_shape=jax.S...  91.3 us

profile of v2, /device:TPU:1, one launch (start us, length us, event | category | flops | bytes accessed | tf_op | source)
XLA Modules:
  0.0 93.0 jit_solution(16834396483524563058)
XLA Ops:
  0.0 91.3 %shard_map.73 = bf16[256,512]{1,0:T(8,128)(2,1)} custom-call(bf16[256,2048]{1,0:T(8,128)(2,1)} %tokens_hbm.1, f32[1,2048]{1,0:T(1,128)} %bitcast.3, s32[4,256]{1,0:T(4,128)} %bitcast.4, f32[4,256]{1,0:T(4,128)} %bitcast.5, bf16[2,2048,512]{2,1,0:T(8,128)(2,1)} %gate_hbm.1, bf16[2,2048,512]{2,1,0:T(8,128)(2,1)} %up_hbm.1, bf16[2,2048,512]{2,1,0:T(8,128)(2,1)} %down_hbm.1), custom_call_target="tpu_custom_call" | custom-call | tf_op jit(solution)/shard_map/pallas_call | solution.py:605
  91.3 1.7 %copy.9 = bf16[256,512]{1,0:T(8,128)(2,1)} copy(bf16[256,512]{1,0:T(8,128)(2,1)} %shard_map.73) | data formatting | bytes 524288

commit v3 on v2

--- a/solution.py
+++ b/solution.py
@@ -90,55 +90,63 @@
     return jnp.sum(picked * route_weights[:, :, None], axis=1).astype(jnp.bfloat16)
 
 
-CUT_EIGHTHS = 6
+CUT_SIXTEENTHS = 10
 STAGES = (
     ("L", 1, 0, 0),
     ("F", 1),
     ("L", 1, 0, 1),
     ("S", 1, 0),
-    ("W", 0),
+    ("L", 1, 1, 0),
     ("F", 2),
     ("L", 1, 1, 1),
-    ("L", 1, 1, 0),
+    ("S", 1, 1),
+    ("X", 2),
+    ("Y", 2),
     ("L", 2, 0, 0),
-    ("W", 2),
-    ("L", 2, 1, 1),
+    ("F", 3),
     ("L", 2, 0, 1),
     ("S", 2, 0),
+    ("Y", 3),
+    ("X", 3),
     ("L", 2, 1, 0),
     ("F", 4),
+    ("L", 2, 1, 1),
+    ("D", 2),
     ("S", 2, 1),
-    ("S", 1, 1),
     ("L", 3, 0, 0),
+    ("X", 4),
+    ("Y", 4),
     ("F", 5),
-    ("W", 4),
-    ("F", 3),
-    ("D", 0),
+    ("R", 2),
     ("L", 3, 0, 1),
+    ("S", 3, 0),
+    ("D", 3),
     ("L", 3, 1, 0),
-    ("W", 5),
-    ("S", 3, 0),
+    ("D", 4),
+    ("X", 5),
+    ("Y", 5),
+    ("F", 6),
     ("L", 3, 1, 1),
-    ("F", 6),
-    ("D", 4),
-    ("D", 2),
     ("S", 3, 1),
-    ("R", 2),
     ("R", 4),
-    ("W", 3),
     ("D", 5),
-    ("W", 6),
+    ("R", 3),
+    ("X", 6),
+    ("Y", 6),
     ("F", 7),
     ("R", 5),
-    ("D", 3),
     ("D", 6),
-    ("R", 3),
-    ("W", 7),
-    ("W", 1),
+    ("X", 7),
+    ("X", 1),
+    ("Y", 7),
+    ("Y", 1),
+    ("X", 0),
+    ("Y", 0),
     ("R", 6),
     ("D", 7),
     ("R", 7),
     ("D", 1),
+    ("D", 0),
     ("R", 1),
 )
 
@@ -199,7 +207,7 @@
     quarter = toks.shape[4]
     out_cols = down_w.shape[2]
     half_rows = tok_rows // 2
-    cut = tok_rows * CUT_EIGHTHS // 8
+    cut = tok_rows * CUT_SIXTEENTHS // 16
     me = lax.axis_index("ep")
     tp = lax.axis_index("tp")
     z, core = me // 2, me % 2
@@ -258,10 +266,12 @@
         pltpu.make_async_copy(ids_hbm, ids_in.at[me], local_sem.at[1]),
         pltpu.make_async_copy(mix_hbm, mix_in.at[me], local_sem.at[2]),
     ]
-    loads = [
-        pltpu.make_async_copy(hbm, vmem, weight_sem.at[n])
-        for n, (hbm, vmem) in enumerate(((gate_hbm, gate_w), (up_hbm, up_w), (down_hbm, down_w)))
-    ]
+    tables = ((gate_hbm, gate_w), (up_hbm, up_w), (down_hbm, down_w))
+
+    def load(w, n):
+        hbm, vmem = tables[w]
+        return pltpu.make_async_copy(hbm.at[n], vmem.at[n], weight_sem.at[w, n])
+
     for copy in small + tok_loads:
         copy.start()
 
@@ -285,8 +295,8 @@
 
     for copy in small + tok_loads:
         copy.wait()
-    for copy in loads:
-        copy.start()
+    load(0, 0).start()
+    load(1, 0).start()
     band = 32
 
     @pl.loop(0, piece_count)
@@ -300,6 +310,9 @@
             for q in range(4):
                 toks[me, q // 2, q % 2, at, :] = normal[:, q * quarter : (q + 1) * quarter]
 
+    for n in range(1, local_count):
+        load(0, n).start()
+        load(1, n).start()
     pending = []
 
     def go(copy):
@@ -359,7 +372,6 @@
     )
     own_copies = []
     metas = []
-    acts_sent = {}
 
     def run_start():
         pl.semaphore_wait(barrier, sources + 1)
@@ -385,18 +397,32 @@
         def _():
             start_line(0)
 
-        own_copies[0].wait_recv()
-        own_copies[1].wait_recv()
-
         @pl.when(core == 1)
         def _():
+            own_copies[0].wait_recv()
+            own_copies[1].wait_recv()
             start_line(0)
-
-        start_line(1)
+            start_line(1)
+
+        make_meta(me)
+        compute_act(0)
+        send_act(0)
+        for n in range(local_count):
+            load(2, n).start()
+
+        @pl.when(core == 0)
+        def _():
+            own_copies[0].wait_recv()
+            own_copies[1].wait_recv()
+            start_line(1)
+
         for up, there in ends:
             for i in range(2):
                 for e in range(parts):
                     always(there, line(z, i, e, up))
+        for n in range(local_count):
+            load(2, n).wait()
+
     def run_line(distance, i, e):
         for up, chip in ((1, z - distance), (0, z + distance)):
             here = chip >= 0 if up else chip < chips
@@ -457,6 +483,9 @@
 
         @pl.loop(0, local_count)
         def _(n):
+            if s == 0:
+                load(0, n).wait()
+                load(1, n).wait()
             block = rows[n]
             half = units // 2
             for part in range(2):
@@ -464,13 +493,34 @@
                 gate = jnp.dot(block, gate_w[n, :, cols], preferred_element_type=jnp.float32)
                 up = jnp.dot(block, up_w[n, :, cols], preferred_element_type=jnp.float32)
                 acts[s, tp, n, :, cols] = clamped_units(gate, up).astype(jnp.bfloat16)
+            own_act(s, n, 0).start()
+
+    def own_act(s, n, along):
+        piece = acts.at[s, tp, n]
+        return remote(
+            piece,
+            piece,
+            act_send.at[s, along, n],
+            act_recv.at[s, along, n],
+            place(me, (tp_x, tp_y)[along]),
+        )
+
+    def passed_act(s, along):
+        n = 1 - along
+        piece = acts.at[s, (tp_y, tp_x)[along], n]
+        return remote(
+            piece,
+            piece,
+            act_send.at[s, along, 2],
+            act_recv.at[s, along, 2],
+            place(me, (tp_x, tp_y)[along]),
+        )
 
     def send_act(s):
-        piece = acts.at[s, tp]
-        acts_sent[s] = [
-            go(remote(piece, piece, act_send.at[s, n], act_recv.at[s, n], place(me, column)))
-            for n, column in enumerate((tp_x, tp_y))
-        ]
+        for n in range(local_count):
+            pending.append(own_act(s, n, 0))
+        for n in reversed(range(local_count)):
+            go(own_act(s, n, 1))
 
     def run_first(s):
         while metas:
@@ -485,26 +535,21 @@
         compute_act(s)
         send_act(s)
 
-    def run_forward(s):
-        mid = local_count // 2
-        for n, (origin, column, at, size) in enumerate(
-            ((tp_x, tp_y, 0, mid), (tp_y, tp_x, mid, local_count - mid))
-        ):
-            acts_sent[s][n].wait_recv()
-            piece = acts.at[s, origin, pl.ds(at, size)]
-            acts_sent[s].append(
-                go(
-                    remote(
-                        piece, piece, act_send.at[s, 2 + n], act_recv.at[s, 2 + n], place(me, column)
-                    )
-                )
-            )
+    def pass_to_y(s):
+        own_act(s, 0, 0).wait_recv()
+        go(passed_act(s, 1))
+
+    def pass_to_x(s):
+        own_act(s, 1, 1).wait_recv()
+        go(passed_act(s, 0))
 
     pairs = {}
 
     def run_second(s):
-        acts_sent[s][2].wait_recv()
-        acts_sent[s][3].wait_recv()
+        own_act(s, 1, 0).wait_recv()
+        own_act(s, 0, 1).wait_recv()
+        passed_act(s, 0).wait_recv()
+        passed_act(s, 1).wait_recv()
 
         @pl.loop(0, local_count)
         def _(n):
@@ -552,17 +597,12 @@
             )
 
     run_start()
-    make_meta(me)
-    loads[0].wait()
-    loads[1].wait()
-    compute_act(0)
-    send_act(0)
-    loads[2].wait()
     runs = {
         "L": run_line,
         "S": run_side,
         "F": run_first,
-        "W": run_forward,
+        "X": pass_to_y,
+        "Y": pass_to_x,
         "D": run_second,
         "R": run_back,
     }
@@ -626,7 +666,7 @@
             pltpu.VMEM((chips, 2, half_rows, out_cols), bf16),
             pltpu.VMEM((chips, 2, half_rows, out_cols), bf16),
             pltpu.VMEM((chips, 2, half_rows, out_cols), bf16),
-            dma((3,)),
+            dma((3, local_count)),
             dma((4,)),
             dma((3,)),
             dma((2, sources)),
@@ -639,8 +679,8 @@
             dma((chips, 2)),
             dma((chips, 2, 3)),
             dma((chips, 2, 3)),
-            dma((sources, 4)),
-            dma((sources, 4)),
+            dma((sources, 2, 3)),
+            dma((sources, 2, 3)),
             dma((sources,)),
             dma((sources,)),
             dma((chips, 2)),
@@ -664,7 +704,7 @@
             tp_count == 4
             and sources == 8
             and capacity % 16 == 0
-            and w_gate.shape[0] in (2, 4, 6, 8)
+            and w_gate.shape[0] == 2
             and tok_rows % 128 == 0
             and tokens.shape[1] % 512 == 0
             and gathered < 32 * 1024 * 1024

time: 93.1 us -> 87.5 us (0.940)
  Pallas kernels: 91.3 us -> 85.7 us
    pallas_call x1, Pallas kernels: 91.3 us -> 85.7 us  [fused_per_device(): pl.pallas_call(functools.partial(layer_kernel, capacity), out_shape=jax.S...]
where the time goes in v3:
time: 87.5 us; the launch traced here: 87.4 us
  Pallas kernels  85.7 us (98%)
  local copies, waits for them, and re-layouts  1.67 us (2%)
    pallas_call x1, Pallas kernels, fused_per_device(): pl.pallas_call(functools.partial(layer_kernel, capacity), out_shape=jax.S...  85.7 us

profile of v3, /device:TPU:1, one launch (start us, length us, event | category | flops | bytes accessed | tf_op | source)
XLA Modules:
  0.0 87.4 jit_solution(15352242610368127425)
XLA Ops:
  0.0 85.7 %shard_map.73 = bf16[256,512]{1,0:T(8,128)(2,1)} custom-call(bf16[256,2048]{1,0:T(8,128)(2,1)} %tokens_hbm.1, f32[1,2048]{1,0:T(1,128)} %bitcast.3, s32[4,256]{1,0:T(4,128)} %bitcast.4, f32[4,256]{1,0:T(4,128)} %bitcast.5, bf16[2,2048,512]{2,1,0:T(8,128)(2,1)} %gate_hbm.1, bf16[2,2048,512]{2,1,0:T(8,128)(2,1)} %up_hbm.1, bf16[2,2048,512]{2,1,0:T(8,128)(2,1)} %down_hbm.1), custom_call_target="tpu_custom_call" | custom-call | tf_op jit(solution)/shard_map/pallas_call | solution.py:645
  85.7 1.7 %copy.9 = bf16[256,512]{1,0:T(8,128)(2,1)} copy(bf16[256,512]{1,0:T(8,128)(2,1)} %shard_map.73) | data formatting | bytes 524288

commit v4 on v3

--- a/solution.py
+++ b/solution.py
@@ -184,7 +184,6 @@
     local_sem,
     meta_send,
     meta_recv,
-    own_send,
     own_recv,
     line_send,
     line_recv,
@@ -251,16 +250,7 @@
             barrier, inc=1, device_id=place(me, column), device_id_type=pl.DeviceIdType.MESH
         )
 
-    piece_count = tok_sem.shape[0]
-    piece_rows = tok_rows // piece_count
-    tok_loads = [
-        pltpu.make_async_copy(
-            tokens_hbm.at[pl.ds(n * piece_rows, piece_rows)],
-            tok_in.at[pl.ds(n * piece_rows, piece_rows)],
-            tok_sem.at[n],
-        )
-        for n in range(piece_count)
-    ]
+    tok_loads = [pltpu.make_async_copy(tokens_hbm, tok_in, tok_sem.at[0])]
     small = [
         pltpu.make_async_copy(gain_hbm, gain_in, local_sem.at[0]),
         pltpu.make_async_copy(ids_hbm, ids_in.at[me], local_sem.at[1]),
@@ -299,10 +289,10 @@
     load(1, 0).start()
     band = 32
 
-    @pl.loop(0, piece_count)
+    @pl.loop(0, tok_rows // (2 * band))
     def _(p):
-        for n in range(piece_rows // band):
-            at = pl.ds(pl.multiple_of(p * piece_rows + n * band, band), band)
+        for n in range(2):
+            at = pl.ds(pl.multiple_of((2 * p + n) * band, band), band)
             values = tok_in[at, :].astype(jnp.float32)
             centred = values - jnp.mean(values, axis=1, keepdims=True)
             row_var = jnp.mean(centred * centred, axis=1, keepdims=True)
@@ -313,15 +303,15 @@
     for n in range(1, local_count):
         load(0, n).start()
         load(1, n).start()
-    pending = []
-
     def go(copy):
         copy.start()
-        pending.append(copy)
         return copy
 
-    def always(condition, copy):
-        pending.append((condition, copy))
+    def all_sent(piece, semaphore):
+        remote(piece, piece, semaphore, back_recv.at[0], place(mate, tp)).wait_send()
+
+    def all_here(piece, semaphore):
+        remote(piece, piece, back_send.at[0], semaphore, place(mate, tp)).wait_recv()
 
     def line(chip, i, e, up):
         source = chip * 2 + i
@@ -332,7 +322,7 @@
         return remote(
             piece,
             piece,
-            line_send.at[up, chip, i, e],
+            line_send.at[up, e],
             line_recv.at[chip, i, e],
             place((z + 2 * up - 1) * 2 + core, tp),
         )
@@ -340,7 +330,7 @@
     def side(chip, i):
         piece = toks.at[chip * 2 + i, own_half, core, pl.ds(0, cut)]
         return remote(
-            piece, piece, side_send.at[chip, i], side_recv.at[chip, i], place(me, side_tp)
+            piece, piece, side_send.at[0], side_recv.at[chip, i], place(me, side_tp)
         )
 
     def to_mate(chip, i, m):
@@ -351,10 +341,9 @@
             toks.at[source, 1 - own_half, core, pl.ds(0, cut)],
         )[m]
         return remote(
-            piece, piece, mate_send.at[chip, i, m], mate_recv.at[chip, i, m], place(mate, tp)
-        )
-
-    mate_parts = (0, 1, 2) if parts > 1 else (0, 2)
+            piece, piece, mate_send.at[0], mate_recv.at[chip, i], place(mate, tp)
+        )
+
     ends = ((1, z < chips - 1), (0, z > 0))
 
     def start_line(i):
@@ -382,15 +371,15 @@
                         remote(
                             table.at[me],
                             table.at[me],
-                            meta_send.at[n, d],
-                            meta_recv.at[n, d],
+                            meta_send.at[n],
+                            meta_recv.at[n],
                             place((me + d) % sources, tp),
                         )
                     )
                 )
         for n, piece in enumerate(own_pieces):
             own_copies.append(
-                go(remote(piece, piece, own_send.at[n], own_recv.at[n], place(mate, tp)))
+                go(remote(piece, piece, mate_send.at[0], own_recv.at[n], place(mate, tp)))
             )
 
         @pl.when(core == 0)
@@ -416,10 +405,6 @@
             own_copies[1].wait_recv()
             start_line(1)
 
-        for up, there in ends:
-            for i in range(2):
-                for e in range(parts):
-                    always(there, line(z, i, e, up))
         for n in range(local_count):
             load(2, n).wait()
 
@@ -427,7 +412,6 @@
         for up, chip in ((1, z - distance), (0, z + distance)):
             here = chip >= 0 if up else chip < chips
             ahead = z + 2 * up - 1
-            onward = jnp.logical_and(here, ahead < chips if up else ahead >= 0)
 
             @pl.when(here)
             def _():
@@ -441,10 +425,6 @@
                     side(chip, i).start()
                 to_mate(chip, i, e).start()
 
-            always(onward, line(chip, i, e, up))
-            if e == 0:
-                always(here, side(chip, i))
-            always(here, to_mate(chip, i, e))
 
     def run_side(k, i):
         chip = partner(k)
@@ -500,8 +480,8 @@
         return remote(
             piece,
             piece,
-            act_send.at[s, along, n],
-            act_recv.at[s, along, n],
+            act_send.at[0],
+            act_recv.at[s, 2 - (2 - along) * (1 - (n - along) * (n - along))],
             place(me, (tp_x, tp_y)[along]),
         )
 
@@ -511,27 +491,26 @@
         return remote(
             piece,
             piece,
-            act_send.at[s, along, 2],
-            act_recv.at[s, along, 2],
+            act_send.at[0],
+            act_recv.at[s, 2],
             place(me, (tp_x, tp_y)[along]),
         )
 
     def send_act(s):
-        for n in range(local_count):
-            pending.append(own_act(s, n, 0))
         for n in reversed(range(local_count)):
             go(own_act(s, n, 1))
 
     def run_first(s):
-        while metas:
-            metas.pop().wait_recv()
+        if metas:
+            all_here(ids_in.at[pl.ds(0, sources - 1)], meta_recv.at[0])
+            all_here(mix_in.at[pl.ds(0, sources - 1)], meta_recv.at[1])
+            metas.clear()
         make_meta(source_of(s))
         if s == 1:
             own_copies[2].wait_recv()
         elif s > 1:
             chip = partner(s // 2)
-            for m in mate_parts:
-                to_mate(chip, s % 2, m).wait_recv()
+            all_here(toks.at[chip * 2 + s % 2, :, core], mate_recv.at[chip, s % 2])
         compute_act(s)
         send_act(s)
 
@@ -546,10 +525,7 @@
     pairs = {}
 
     def run_second(s):
-        own_act(s, 1, 0).wait_recv()
-        own_act(s, 0, 1).wait_recv()
-        passed_act(s, 0).wait_recv()
-        passed_act(s, 1).wait_recv()
+        all_here(acts.at[s, pl.ds(0, 2)], act_recv.at[s, 2])
 
         @pl.loop(0, local_count)
         def _(n):
@@ -578,7 +554,7 @@
             pair_out[s // 2, s % 2] = combined[s, 1 - core].astype(jnp.bfloat16)
             piece, target = pair_out.at[s // 2, s % 2], pair_in.at[s // 2, s % 2]
         if s > 0:
-            pairs[s] = go(remote(piece, target, pair_send.at[s], pair_recv.at[s], place(mate, tp)))
+            pairs[s] = go(remote(piece, target, pair_send.at[0], pair_recv.at[s], place(mate, tp)))
 
     def run_back(s):
         pairs[s].wait_recv()
@@ -590,8 +566,8 @@
                 remote(
                     back_out.at[k, i],
                     back_in.at[z, core],
-                    back_send.at[k, i],
-                    back_recv.at[z, core],
+                    back_send.at[0],
+                    back_recv.at[0],
                     place(partner(k) * 2 + i, tp),
                 )
             )
@@ -608,23 +584,32 @@
     }
     for kind, *rest in STAGES:
         runs[kind](*rest)
+    all_here(back_in.at[pl.ds(0, chips - 1)], back_recv.at[0])
     for h in range(2):
         result = combined[0, h] + pair_in[0, h].astype(jnp.float32)
         for d in range(1, chips):
-            chip = (z + d) % chips
-            remote(
-                back_out.at[0, 0], back_in.at[chip, h], back_send.at[0, h], back_recv.at[chip, h], place(mate, tp)
-            ).wait_recv()
-            result = result + back_in[chip, h].astype(jnp.float32)
+            result = result + back_in[(z + d) % chips, h].astype(jnp.float32)
         out_ref[h * half_rows : (h + 1) * half_rows, :] = result.astype(out_ref.dtype)
-    for entry in pending:
-        if isinstance(entry, tuple):
-
-            @pl.when(entry[0])
-            def _():
-                entry[1].wait_send()
-        else:
-            entry.wait_send()
+    all_sent(ids_in.at[pl.ds(0, sources - 1)], meta_send.at[0])
+    all_sent(mix_in.at[pl.ds(0, sources - 1)], meta_send.at[1])
+    all_sent(toks.at[pl.ds(0, chips)], mate_send.at[0])
+    all_sent(toks.at[pl.ds(0, 2 * chips - 2), 0, 0, pl.ds(0, cut)], side_send.at[0])
+    all_sent(acts.at[pl.ds(0, 3 * sources // 4)], act_send.at[0])
+    all_sent(pair_out, pair_send.at[0])
+    all_sent(back_out.at[pl.ds(1, chips - 1)], back_send.at[0])
+    for at in range(chips):
+
+        @pl.when(z == at)
+        def _():
+            for up, chip_count in ((1, at + 1), (0, chips - at)):
+                if chip_count == chips:
+                    continue
+                for e in range(parts):
+                    first, size = ((0, tok_rows), (cut, tok_rows - cut))[e]
+                    all_sent(
+                        toks.at[pl.ds(0, 2 * chip_count), 0, 0, pl.ds(first, size)],
+                        line_send.at[up, e],
+                    )
 
 
 def fused_per_device(tokens, norm_gain, route_ids, route_weights, w_gate, w_up, w_down):
@@ -644,7 +629,7 @@
     hbm = pl.BlockSpec(memory_space=pltpu.HBM)
     return pl.pallas_call(
         functools.partial(layer_kernel, capacity),
-        out_shape=jax.ShapeDtypeStruct((tok_rows, out_cols), bf16),
+        out_shape=pltpu.VMEM((tok_rows, out_cols), bf16),
         in_specs=[hbm] * 7,
         out_specs=vmem,
         scratch_shapes=[
@@ -667,27 +652,26 @@
             pltpu.VMEM((chips, 2, half_rows, out_cols), bf16),
             pltpu.VMEM((chips, 2, half_rows, out_cols), bf16),
             dma((3, local_count)),
-            dma((4,)),
+            dma((1,)),
             dma((3,)),
-            dma((2, sources)),
-            dma((2, sources)),
+            dma((2,)),
+            dma((2,)),
             dma((3,)),
-            dma((3,)),
-            dma((2, chips, 2, 2)),
+            dma((2, 2)),
             dma((chips, 2, 2)),
+            dma((1,)),
             dma((chips, 2)),
+            dma((1,)),
             dma((chips, 2)),
-            dma((chips, 2, 3)),
-            dma((chips, 2, 3)),
-            dma((sources, 2, 3)),
-            dma((sources, 2, 3)),
+            dma((1,)),
+            dma((sources, 3)),
+            dma((1,)),
             dma((sources,)),
-            dma((sources,)),
-            dma((chips, 2)),
-            dma((chips, 2)),
+            dma((1,)),
+            dma((1,)),
         ],
         compiler_params=pltpu.CompilerParams(
-            collective_id=0, has_side_effects=True, vmem_limit_bytes=60 * 1024 * 1024
+            collective_id=0, has_side_effects=True, vmem_limit_bytes=61 * 1024 * 1024
         ),
     )(tokens, norm_gain.reshape(1, width), route_ids.T, route_weights.T, w_gate, w_up, w_down)
 

time: 87.5 us -> 84.1 us (0.961)
  Pallas kernels: 85.7 us -> 83.2 us
  local copies, waits for them, and re-layouts: 1.67 us -> 0.71 us
    pallas_call x1, Pallas kernels: 85.7 us -> 83.2 us  [fused_per_device(): pl.pallas_call(functools.partial(layer_kernel, capacity), out_shape=pltpu...]
    unnamed x1, local copies, waits for them, and re-layouts: 1.67 us -> 0.71 us
where the time goes in v4:
time: 84.1 us; the launch traced here: 83.9 us
  Pallas kernels  83.2 us (99%)
    pallas_call x1, Pallas kernels, fused_per_device(): pl.pallas_call(functools.partial(layer_kernel, capacity), out_shape=pltpu...  83.2 us

profile of v4, /device:TPU:1, one launch (start us, length us, event | category | flops | bytes accessed | tf_op | source)
XLA Modules:
  0.0 83.9 jit_solution(5397131667487249259)
XLA Ops:
  0.0 83.2 %shard_map.73 = bf16[256,512]{1,0:T(8,128)(2,1)S(1)} custom-call(bf16[256,2048]{1,0:T(8,128)(2,1)} %tokens_hbm.1, f32[1,2048]{1,0:T(1,128)} %bitcast.3, s32[4,256]{1,0:T(4,128)} %bitcast.4, f32[4,256]{1,0:T(4,128)} %bitcast.5, bf16[2,2048,512]{2,1,0:T(8,128)(2,1)} %gate_hbm.1, bf16[2,2048,512]{2,1,0:T(8,128)(2,1)} %up_hbm.1, bf16[2,2048,512]{2,1,0:T(8,128)(2,1)} %down_hbm.1), custom_call_target="tpu_custom_call" | custom-call | tf_op jit(solution)/shard_map/pallas_call | solution.py:630
  83.2 0.7 copy.9

commit v5 on v4

--- a/solution.py
+++ b/solution.py
@@ -92,16 +92,19 @@
 
 CUT_SIXTEENTHS = 10
 STAGES = (
+    ("Y", 0),
     ("L", 1, 0, 0),
     ("F", 1),
     ("L", 1, 0, 1),
+    ("X", 0),
     ("S", 1, 0),
+    ("Y", 1),
     ("L", 1, 1, 0),
     ("F", 2),
     ("L", 1, 1, 1),
     ("S", 1, 1),
+    ("Y", 2),
     ("X", 2),
-    ("Y", 2),
     ("L", 2, 0, 0),
     ("F", 3),
     ("L", 2, 0, 1),
@@ -110,43 +113,40 @@
     ("X", 3),
     ("L", 2, 1, 0),
     ("F", 4),
+    ("D", 2),
+    ("D", 3),
     ("L", 2, 1, 1),
-    ("D", 2),
     ("S", 2, 1),
     ("L", 3, 0, 0),
+    ("Y", 4),
     ("X", 4),
-    ("Y", 4),
     ("F", 5),
-    ("R", 2),
+    ("R", 3),
     ("L", 3, 0, 1),
+    ("D", 0),
     ("S", 3, 0),
-    ("D", 3),
+    ("X", 5),
+    ("Y", 5),
     ("L", 3, 1, 0),
     ("D", 4),
-    ("X", 5),
-    ("Y", 5),
     ("F", 6),
+    ("R", 4),
     ("L", 3, 1, 1),
+    ("D", 5),
     ("S", 3, 1),
-    ("R", 4),
-    ("D", 5),
-    ("R", 3),
+    ("R", 5),
+    ("Y", 6),
     ("X", 6),
-    ("Y", 6),
     ("F", 7),
-    ("R", 5),
     ("D", 6),
     ("X", 7),
     ("X", 1),
     ("Y", 7),
-    ("Y", 1),
-    ("X", 0),
-    ("Y", 0),
     ("R", 6),
+    ("R", 2),
     ("D", 7),
     ("R", 7),
     ("D", 1),
-    ("D", 0),
     ("R", 1),
 )
 
@@ -213,19 +213,14 @@
     y, x = tp // 2, tp % 2
     tp_x = y * 2 + (1 - x)
     tp_y = (1 - y) * 2 + x
-    side_tp = tp_x * (1 - core) + tp_y * core
     mate = z * 2 + (1 - core)
     own_half = (x + y) % 2
     parts = 2 if cut < tok_rows else 1
 
     def partner(k):
-        chosen_chip = 0 * z
-        for at in range(chips):
-            sign = 1 if 2 * at < chips else -1
-            order = sorted(range(chips), key=lambda c: (abs(c - at), sign * c))
-            gap = (z - at) * (z - at)
-            chosen_chip = chosen_chip + order[k] * (1 - (gap + chips * chips - 1) // (chips * chips))
-        return chosen_chip
+        low = (z + k) % 2
+        high = (z // 2 + k // 2) % 2
+        return 2 * high + low
 
     def place(ep, column):
         return {"ep": ep, "tp": column}
@@ -291,6 +286,12 @@
 
     @pl.loop(0, tok_rows // (2 * band))
     def _(p):
+        @pl.when(p == 2)
+        def _():
+            for n in range(1, local_count):
+                load(0, n).start()
+                load(1, n).start()
+
         for n in range(2):
             at = pl.ds(pl.multiple_of((2 * p + n) * band, band), band)
             values = tok_in[at, :].astype(jnp.float32)
@@ -300,9 +301,6 @@
             for q in range(4):
                 toks[me, q // 2, q % 2, at, :] = normal[:, q * quarter : (q + 1) * quarter]
 
-    for n in range(1, local_count):
-        load(0, n).start()
-        load(1, n).start()
     def go(copy):
         copy.start()
         return copy
@@ -327,10 +325,14 @@
             place((z + 2 * up - 1) * 2 + core, tp),
         )
 
-    def side(chip, i):
-        piece = toks.at[chip * 2 + i, own_half, core, pl.ds(0, cut)]
+    def side(chip, i, along):
+        piece = toks.at[chip * 2 + i, own_half, core, pl.ds(along * (cut // 2), cut // 2)]
         return remote(
-            piece, piece, side_send.at[0], side_recv.at[chip, i], place(me, side_tp)
+            piece,
+            piece,
+            side_send.at[0],
+            side_recv.at[chip, i],
+            place(me, (tp_x, tp_y)[along]),
         )
 
     def to_mate(chip, i, m):
@@ -364,6 +366,10 @@
 
     def run_start():
         pl.semaphore_wait(barrier, sources + 1)
+        for n, piece in enumerate(own_pieces):
+            own_copies.append(
+                go(remote(piece, piece, mate_send.at[0], own_recv.at[n], place(mate, tp)))
+            )
         for d in range(1, sources):
             for n, table in enumerate((ids_in, mix_in)):
                 metas.append(
@@ -377,21 +383,9 @@
                         )
                     )
                 )
-        for n, piece in enumerate(own_pieces):
-            own_copies.append(
-                go(remote(piece, piece, mate_send.at[0], own_recv.at[n], place(mate, tp)))
-            )
-
         @pl.when(core == 0)
         def _():
             start_line(0)
-
-        @pl.when(core == 1)
-        def _():
-            own_copies[0].wait_recv()
-            own_copies[1].wait_recv()
-            start_line(0)
-            start_line(1)
 
         make_meta(me)
         compute_act(0)
@@ -399,15 +393,6 @@
         for n in range(local_count):
             load(2, n).start()
 
-        @pl.when(core == 0)
-        def _():
-            own_copies[0].wait_recv()
-            own_copies[1].wait_recv()
-            start_line(1)
-
-        for n in range(local_count):
-            load(2, n).wait()
-
     def run_line(distance, i, e):
         for up, chip in ((1, z - distance), (0, z + distance)):
             here = chip >= 0 if up else chip < chips
@@ -422,13 +407,14 @@
                     line(chip, i, e, up).start()
 
                 if e == 0:
-                    side(chip, i).start()
+                    side(chip, i, 0).start()
+                    side(chip, i, 1).start()
                 to_mate(chip, i, e).start()
 
 
     def run_side(k, i):
         chip = partner(k)
-        side(chip, i).wait_recv()
+        all_here(toks.at[chip * 2 + i, own_half, core, pl.ds(0, cut)], side_recv.at[chip, i])
         go(to_mate(chip, i, 2))
 
     def chosen(source):
@@ -474,6 +460,18 @@
                 up = jnp.dot(block, up_w[n, :, cols], preferred_element_type=jnp.float32)
                 acts[s, tp, n, :, cols] = clamped_units(gate, up).astype(jnp.bfloat16)
             own_act(s, n, 0).start()
+            if s == 0:
+
+                @pl.when(n == 1 - core)
+                def _():
+                    own_copies[0].wait_recv()
+                    own_copies[1].wait_recv()
+
+                    @pl.when(core == 1)
+                    def _():
+                        start_line(0)
+
+                    start_line(1)
 
     def own_act(s, n, along):
         piece = acts.at[s, tp, n]
@@ -523,8 +521,11 @@
         go(passed_act(s, 0))
 
     pairs = {}
+    down_loads = [load(2, n) for n in range(local_count)]
 
     def run_second(s):
+        while down_loads:
+            down_loads.pop().wait()
         all_here(acts.at[s, pl.ds(0, 2)], act_recv.at[s, 2])
 
         @pl.loop(0, local_count)

time: 84.1 us -> 83.4 us (level)
  Pallas kernels: 83.2 us -> 81.7 us
    pallas_call x1, Pallas kernels: 83.2 us -> 81.7 us  [fused_per_device(): pl.pallas_call(functools.partial(layer_kernel, capacity), out_shape=pltpu...]
where the time goes in v5:
time: 83.4 us; the launch traced here: 82.4 us
  Pallas kernels  81.7 us (98%)
    pallas_call x1, Pallas kernels, fused_per_device(): pl.pallas_call(functools.partial(layer_kernel, capacity), out_shape=pltpu...  81.7 us

profile of v5, /device:TPU:1, one launch (start us, length us, event | category | flops | bytes accessed | tf_op | source)
XLA Modules:
  0.0 82.4 jit_solution(8267720666404654074)
XLA Ops:
  0.0 81.7 %shard_map.73 = bf16[256,512]{1,0:T(8,128)(2,1)S(1)} custom-call(bf16[256,2048]{1,0:T(8,128)(2,1)} %tokens_hbm.1, f32[1,2048]{1,0:T(1,128)} %bitcast.3, s32[4,256]{1,0:T(4,128)} %bitcast.4, f32[4,256]{1,0:T(4,128)} %bitcast.5, bf16[2,2048,512]{2,1,0:T(8,128)(2,1)} %gate_hbm.1, bf16[2,2048,512]{2,1,0:T(8,128)(2,1)} %up_hbm.1, bf16[2,2048,512]{2,1,0:T(8,128)(2,1)} %down_hbm.1), custom_call_target="tpu_custom_call" | custom-call | tf_op jit(solution)/shard_map/pallas_call | solution.py:631
  81.7 0.7 copy.9
